TPU v7x, 32 devices: a whole 2x2x4 slice. The times are simulated.
32 devices in a mesh: grp: 2 (over x), ep: 16 (over z, y, core).
Axes of the slice: x: 2, y: 2, z: 4, core: 2. Of those that a mesh axis runs over, the one named last changes fastest.
Arguments:
- hidden: bfloat16 [4096, 2048], P(('grp', 'ep')), parts along dimension 0, may hold values from -6 to 6
- state: float32 [2, 4096, 4096], P(None, ('grp', 'ep')), parts along dimension 1, may hold values from -6 to 6
- norm_gain: float32 [2048], replicated, may hold values from 0.1 to 1.9
- w_in: bfloat16 [2048, 1024], P(None, 'ep'), may hold values from -0.125 to 0.125
- lam_re: float32 [64, 64], replicated, may hold values from -1 to -0.1
- lam_im: float32 [64, 64], replicated, may hold values from 0 to 200
- log_step: float32 [64], replicated, may hold values from -4.6 to -0.7
- in_re: float32 [64, 64, 16], replicated, may hold values from -1 to 1
- in_im: float32 [64, 64, 16], replicated, may hold values from -1 to 1
- out_re: float32 [64, 16, 64], replicated, may hold values from -0.75 to 0.75
- out_im: float32 [64, 16, 64], replicated, may hold values from -0.75 to 0.75
- skip: float32 [1024], replicated, may hold values from -4 to 4
- w_glu: bfloat16 [1024, 1024], replicated, may hold values from -0.1875 to 0.1875
- w_out: bfloat16 [1024, 2048], replicated, may hold values from -0.375 to 0.375
- ffn_gain: float32 [2048], replicated, may hold values from 0.1 to 1.9
- w_group: bfloat16 [2048, 4], replicated, may hold values from -0.03125 to 0.03125
- w_route: bfloat16 [2048, 16], replicated, may hold values from -0.03125 to 0.03125
- w_gate: bfloat16 [16, 2048, 512], P('ep'), may hold values from -0.125 to 0.125
- w_up: bfloat16 [16, 2048, 512], P('ep'), may hold values from -0.125 to 0.125
- w_down: bfloat16 [16, 512, 2048], P('ep'), may hold values from -2 to 2
- route_ids: int32 [4096, 2], P(('grp', 'ep')), parts along dimension 0, may hold values from 0 to 15, as said below
Outputs:
- hidden_out: bfloat16 [4096, 2048], P(('grp', 'ep')), parts along dimension 0
- new_state: float32 [2, 4096, 4096], P(None, ('grp', 'ep')), parts along dimension 1
There are 2 independent parts, one for each index of `grp`. A program takes and returns all parts, laid end to end along the dimension named above; an argument that names none is the same for every part. Nothing has to cross between parts.
Inputs may be any that keep to these rules, and one draw needn't show every extreme that they name: `route_ids`: each row names 2 different experts of one expert group (experts g * 4 to g * 4 + 3). Among the rows of one device no expert is named more than 32 times, and in every draw some experts are named exactly 32 times by the rows of every device.
All inputs are finite; a program needn't handle non-finite values.
Results may differ from a plain program's by a relative error of at most 0.013.
Values may be sent and summed in bfloat16 or wider, within the bound.
A program may use at most 128 MiB of HBM per device.

v0:
```python
import jax
import jax.numpy as jnp
from jax import lax
from jax.sharding import PartitionSpec as P

EXP_GROUPS = 4
EXP_DEV = 1
TOPK = 2


def normalize(rows, gain):
    wide = rows.astype(jnp.float32)
    return wide * lax.rsqrt(jnp.mean(wide * wide, axis=-1, keepdims=True) + 1e-06) * gain


def discretize(lam_re, lam_im, log_step, in_re, in_im):
    step = jnp.exp(log_step)[:, None]
    magnitude = jnp.exp(lam_re * step)
    bar_re = magnitude * jnp.cos(lam_im * step)
    bar_im = magnitude * jnp.sin(lam_im * step)
    denom = lam_re * lam_re + lam_im * lam_im
    lessened = bar_re - 1.0
    coef_re = (lessened * lam_re + bar_im * lam_im) / denom
    coef_im = (bar_im * lam_re - lessened * lam_im) / denom
    drive_re = coef_re[:, :, None] * in_re - coef_im[:, :, None] * in_im
    drive_im = coef_re[:, :, None] * in_im + coef_im[:, :, None] * in_re
    return (bar_re, bar_im, drive_re, drive_im)


def mixer_step(inputs, state, lam_re, lam_im, log_step, in_re, in_im, out_re, out_im, skip, w_glu):
    rows = inputs.shape[0]
    groups, entries = lam_re.shape
    width = in_re.shape[2]
    highest = lax.Precision.HIGHEST
    bar_re, bar_im, drive_re, drive_im = discretize(lam_re, lam_im, log_step, in_re, in_im)
    wide = inputs.astype(jnp.float32)
    grouped = wide.reshape(rows, groups, width)
    push_re = jnp.einsum("bgc,gnc->bgn", grouped, drive_re, precision=highest)
    push_im = jnp.einsum("bgc,gnc->bgn", grouped, drive_im, precision=highest)
    old_re = state[0].reshape(rows, groups, entries)
    old_im = state[1].reshape(rows, groups, entries)
    new_re = bar_re * old_re - bar_im * old_im + push_re
    new_im = bar_re * old_im + bar_im * old_re + push_im
    read = jnp.einsum("bgn,gcn->bgc", new_re, out_re, precision=highest) - jnp.einsum(
        "bgn,gcn->bgc", new_im, out_im, precision=highest
    )
    mixed = read.reshape(rows, groups * width) + skip * wide
    active = jax.nn.gelu(mixed)
    gating = jnp.dot(active.astype(jnp.bfloat16), w_glu, preferred_element_type=jnp.float32)
    result = (active * jax.nn.sigmoid(gating)).astype(jnp.bfloat16)
    new_state = jnp.stack([new_re.reshape(rows, -1), new_im.reshape(rows, -1)])
    return (result, new_state)


def route_gates(normed, w_group, w_route, route_ids, per_group):
    group_logit = jnp.dot(normed, w_group, preferred_element_type=jnp.float32)
    route_logit = jnp.dot(normed, w_route, preferred_element_type=jnp.float32)
    chosen = route_ids[:, 0] // per_group
    pick_group = (
        chosen[:, None] == jnp.arange(group_logit.shape[1], dtype=jnp.int32)[None, :]
    ).astype(jnp.float32)
    own = jnp.sum(group_logit * pick_group, axis=1, keepdims=True)
    group_weight = 1.0 / jnp.sum(jnp.exp(group_logit - own), axis=1)
    pick = (
        route_ids[:, :, None] == jnp.arange(route_logit.shape[1], dtype=jnp.int32)[None, None, :]
    ).astype(jnp.float32)
    chosen_logit = jnp.sum(pick * route_logit[:, None, :], axis=2)
    first = jax.nn.sigmoid(chosen_logit[:, 0] - chosen_logit[:, 1])
    pair = jnp.stack([first, 1.0 - first], axis=1)
    return group_weight[:, None] * pair


def on_device(
    hidden,
    state,
    norm_gain,
    w_in,
    lam_re,
    lam_im,
    log_step,
    in_re,
    in_im,
    out_re,
    out_im,
    skip,
    w_glu,
    w_out,
    ffn_gain,
    w_group,
    w_route,
    w_gate,
    w_up,
    w_down,
    route_ids,
):
    normed = normalize(hidden, norm_gain).astype(jnp.bfloat16)
    inputs = jnp.dot(
        normed, lax.all_gather(w_in, "ep", axis=1, tiled=True), preferred_element_type=jnp.float32
    ).astype(jnp.bfloat16)
    glu, new_state = mixer_step(
        inputs, state, lam_re, lam_im, log_step, in_re, in_im, out_re, out_im, skip, w_glu
    )
    resid = (
        hidden.astype(jnp.float32) + jnp.dot(glu, w_out, preferred_element_type=jnp.float32)
    ).astype(jnp.bfloat16)
    normed2 = normalize(resid, ffn_gain).astype(jnp.bfloat16)
    experts = w_route.shape[1]
    gates = route_gates(normed2, w_group, w_route, route_ids, experts // EXP_GROUPS)
    count_dev = normed2.shape[0]
    model_width = normed2.shape[1]
    capacity = 2 * TOPK * count_dev // experts
    flat = route_ids.reshape(-1)
    hits = (flat[:, None] == jnp.arange(experts, dtype=jnp.int32)[None, :]).astype(jnp.int32)
    before = jnp.sum((jnp.cumsum(hits, axis=0) - hits) * hits, axis=1)
    slot = flat * capacity + before
    place = (slot[:, None] == jnp.arange(experts * capacity, dtype=jnp.int32)[None, :]).astype(
        jnp.bfloat16
    )
    dispatch = jnp.sum(place.reshape(count_dev, TOPK, experts * capacity), axis=1)
    outgoing = jnp.einsum("rs,rd->sd", dispatch, normed2, preferred_element_type=jnp.float32)
    outgoing = outgoing.astype(jnp.bfloat16).reshape(experts, capacity, model_width)
    sources = lax.axis_size("ep")
    received = lax.all_to_all(outgoing, "ep", split_axis=0, concat_axis=0, tiled=True)
    items = received.shape[1]
    arranged = received.reshape(sources, EXP_DEV, items, model_width).transpose(1, 0, 2, 3)
    arranged = arranged.reshape(EXP_DEV, sources * items, model_width)
    gate = jnp.einsum("erd,edf->erf", arranged, w_gate, preferred_element_type=jnp.float32)
    upper = jnp.einsum("erd,edf->erf", arranged, w_up, preferred_element_type=jnp.float32)
    inner = (jax.nn.silu(gate) * upper).astype(jnp.bfloat16)
    result = jnp.einsum("erf,efd->erd", inner, w_down, preferred_element_type=jnp.float32).astype(
        jnp.bfloat16
    )
    result = result.reshape(EXP_DEV, sources, items, model_width).transpose(1, 0, 2, 3)
    result = result.reshape(sources * EXP_DEV, items, model_width)
    returned = lax.all_to_all(result, "ep", split_axis=0, concat_axis=0, tiled=True)
    picked = returned.reshape(experts * capacity, model_width)[slot].reshape(
        count_dev, TOPK, model_width
    )
    moe = jnp.sum(picked.astype(jnp.float32) * gates[:, :, None], axis=1)
    hidden_out = (resid.astype(jnp.float32) + moe).astype(jnp.bfloat16)
    return (hidden_out, new_state)


def solution(mesh):
    return jax.shard_map(
        on_device,
        mesh=mesh,
        in_specs=(
            P(("grp", "ep"), None),
            P(None, ("grp", "ep"), None),
            P(),
            P(None, "ep"),
            P(),
            P(),
            P(),
            P(),
            P(),
            P(),
            P(),
            P(),
            P(),
            P(),
            P(),
            P(),
            P(),
            P("ep", None, None),
            P("ep", None, None),
            P("ep", None, None),
            P(("grp", "ep"), None),
        ),
        out_specs=(P(("grp", "ep"), None), P(None, ("grp", "ep"), None)),
        check_vma=False,
    )
```

profile of v0, /device:TPU:13, one launch (start us, length us, event | category | flops | bytes accessed | tf_op | source)
XLA Modules:
  0.0 221.1 jit_solution(17480860268676464589)
XLA Ops:
  7.2 0.0 copy-start
  7.2 0.0 all-gather.2.cloned.1.call-start
  7.2 0.7 all-gather.2.cloned.1.call-update
  7.9 0.8 copy.62
  8.7 0.1 eq.71
  8.8 0.1 eq.67
  9.0 0.7 exp.22
  9.7 0.6 reduce-window.6
  10.2 0.2 slice_reduce_fusion
  10.5 0.1 fusion.63
  10.6 0.1 reduce_sum.81
  10.7 0.6 broadcast_multiply_fusion
  11.3 0.1 copy.66
  11.4 4.7 %fusion.76 = (f32[1,128,4096]{2,1,0:T(8,128)}, f32[1,128,4096]{2,1,0:T(8,128)}) fusion(f32[2,128,4096]{2,1,0:T(8,128)} %param.22), kind=kLoop, calls=%fused_computation.103 | loop fusion | bytes 8388608 | tf_op jit(solution)/shard_map/slice | solution.py:40
  16.1 2.9 %copy.58 = f32[1,128,4096]{1,2,0:T(8,128)} copy(f32[1,128,4096]{2,1,0:T(8,128)} %get-tuple-element.4) | data formatting | bytes 4194304 | tf_op jit(solution)/shard_map/slice | solution.py:40
  19.1 3.0 %copy.59 = f32[1,128,4096]{1,2,0:T(8,128)} copy(f32[1,128,4096]{2,1,0:T(8,128)} %get-tuple-element.5) | data formatting | bytes 4194304 | tf_op jit(solution)/shard_map/slice | solution.py:41
  22.0 0.1 fusion.41
  22.2 0.2 fusion.18
  22.4 0.9 fusion.60
  23.3 38.0 %all-gather.2.cloned.1.call-done = bf16[2048,1024]{0,1:T(8,128)(2,1)} async-done(((bf16[2048,64]{0,1:T(8,128)(2,1)}), bf16[2048,1024]{0,1:T(8,128)(2,1)}) %all-gather.2.cloned.1.call-update) | async-done | bytes 4194320 | tf_op jit(solution)/shard_map/all_gather | solution.py:98
  61.2 4.4 %convolution_convert_fusion.2 = bf16[128,1024]{1,0:T(8,128)(2,1)} fusion(bf16[2048,1024]{0,1:T(8,128)(2,1)} %all-gather.2.cloned.1.call-done, bf16[128,2048]{1,0:T(8,128)(2,1)S(1)} %copy-done.6, f32[2048]{0:T(1024)S(1)} %copy-done.22, f32[128]{0:T(128)S(1)} %add_rsqrt_fusion.1), kind=kOutput, calls=%fused_computation.26 | convolution fusion | flops 538050560 | bytes 4989440 | tf_op jit(solution)/shard_map/dot_general | solution.py:97
  65.6 1.1 copy.60
  66.8 0.0 copy-start.4
  66.8 4.9 %bitcast_add_fusion = f32[128,64,64]{0,2,1:T(8,128)S(1)} fusion(f32[128,64,64]{0,2,1:T(8,128)} %bitcast.73, f32[128,64,64]{0,2,1:T(8,128)} %bitcast.75, bf16[128,64,16]{0,2,1:T(8,128)(2,1)S(1)} %bitcast.78, f32[64,64]{1,0:T(8,128)} %get-tuple-element.7, f32[64,64]{1,0:T(8,128)} %get-tuple-element.8, f32[64,64,16]{1,2,0:T(8,128)} %param.28, ...), kind=kOutput, calls=%fused_computation.12 | convolution fusion | flops 102957056 | bytes 7143424 | tf_op jit(solution)/shard_map/bgc,gnc->bgn/dot_general | solution.py:39
  71.8 3.2 %bitcast_add_fusion.1 = f32[128,64,64]{0,2,1:T(8,128)S(1)} fusion(f32[128,64,64]{0,2,1:T(8,128)S(1)} %bitcast.76, f32[128,64,64]{0,2,1:T(8,128)S(1)} %bitcast.74, bf16[128,64,16]{0,2,1:T(8,128)(2,1)S(1)} %bitcast.79, f32[64,64]{1,0:T(8,128)S(1)} %copy-done.14, f32[64,64]{1,0:T(8,128)S(1)} %copy-done.15, f32[64,64,16]{1,2,0:T(8,128)S(1)} %copy-done.8, ...), kind=kOutput, calls=%fused_computation.13 | convolution fusion | flops 102957056 | bytes 7143424 | tf_op jit(solution)/shard_map/bgc,gnc->bgn/dot_general | solution.py:38
  75.1 1.9 fusion.79
  77.0 1.9 convolution_subtract_fusion
  78.9 1.0 copy.61
  79.9 5.6 %multiply_reduce_fusion.1 = (f32[128]{0:T(128)S(1)}, f32[128,2048]{1,0:T(8,128)}) fusion(bf16[1024,2048]{1,0:T(8,128)(2,1)} %param.34, bf16[1024,1024]{1,0:T(8,128)(2,1)} %param.33, f32[128,1024]{1,0:T(8,128)} %copy.61, bf16[128,1024]{1,0:T(8,128)(2,1)S(1)} %copy-done.10, f32[1024]{0:T(1024)S(1)} %copy-done.26, bf16[128,2048]{1,0:T(8,128)(2,1)S(1)} %copy-done.6), kind=kOutput, calls=%fused_computation.32 | convolution fusion | flops 810549120 | bytes 8655360 | tf_op jit(solution)/shard_map/dot_general | solution.py:104
  85.6 1.4 multiply_convert_fusion
  87.0 0.7 convolution_convert_fusion
  87.7 51.6 %all_to_all.10 = bf16[16,32,2048]{2,1,0:T(8,128)(2,1)S(1)} all-to-all(bf16[16,32,2048]{2,1,0:T(8,128)(2,1)S(1)} %bitcast.77), channel_id=1, replica_groups=mesh['grp'=2,'ep'=16] {'ep'}, dimensions={0} | all-to-all | bytes 4194304 | tf_op jit(solution)/shard_map/all_to_all | solution.py:123
  139.3 1.3 copy-done.7
  140.7 2.2 %fusion.5 = f32[512,512]{1,0:T(8,128)} fusion(bf16[512,2048]{1,0:T(8,128)(2,1)S(1)} %bitcast.82, bf16[1,2048,512]{2,1,0:T(8,128)(2,1)S(1)} %copy-done.25), kind=kOutput, calls=%fused_computation.10 | convolution fusion | flops 1073741824 | bytes 5242880 | tf_op jit(solution)/shard_map/erd,edf->erf/dot_general | solution.py:127
  142.9 6.2 %convolution_convert_fusion.1 = bf16[512,2048]{1,0:T(8,128)(2,1)} fusion(bf16[1,512,2048]{2,1,0:T(8,128)(2,1)S(1)} %copy-done, bf16[512,2048]{1,0:T(8,128)(2,1)} %bitcast.83, bf16[1,2048,512]{2,1,0:T(8,128)(2,1)} %param.39, f32[512,512]{1,0:T(8,128)} %fusion.5), kind=kOutput, calls=%fused_computation.3 | convolution fusion | flops 2150105088 | bytes 9437184 | tf_op jit(solution)/shard_map/erf,efd->erd/dot_general | solution.py:130
  149.1 5.2 %all-to-all-start.1 = ((bf16[16,32,2048]{2,1,0:T(8,128)(2,1)}), bf16[16,32,2048]{2,1,0:T(8,128)(2,1)}, u32[]{:S(2)}, u32[]{:S(2)}) async-start(bf16[16,32,2048]{2,1,0:T(8,128)(2,1)} %bitcast.81), calls=%async_computation.1 | async-start | bytes 4194304 | tf_op jit(solution)/shard_map/all_to_all | solution.py:135
  154.3 0.1 mul.278
  154.5 0.3 select_reduce_fusion.1
  154.8 0.2 fusion.80
  155.1 0.1 copy.67
  155.2 2.9 %copy.69 = f32[1,128,4096]{2,1,0:T(8,128)} copy(f32[1,128,4096]{1,2,0:T(8,128)} %bitcast.72) | data formatting | bytes 4194304 | tf_op jit(solution)/shard_map/stack;reshape | solution.py:51
  158.2 2.9 %copy.68 = f32[1,128,4096]{2,1,0:T(8,128)} copy(f32[1,128,4096]{1,2,0:T(8,128)} %bitcast.71) | data formatting | bytes 4194304 | tf_op jit(solution)/shard_map/stack;reshape | solution.py:51
  161.1 4.7 %pad_maximum_fusion = f32[2,128,4096]{2,1,0:T(8,128)} fusion(f32[1,128,4096]{2,1,0:T(8,128)} %copy.69, f32[1,128,4096]{2,1,0:T(8,128)} %copy.68), kind=kLoop, calls=%fused_computation.1 | loop fusion | flops 1048576 | bytes 8388608 | tf_op jit(solution)/shard_map/stack | solution.py:51
  165.8 36.1 %all-to-all-done.1 = bf16[16,32,2048]{2,1,0:T(8,128)(2,1)} async-done(((bf16[16,32,2048]{2,1,0:T(8,128)(2,1)}), bf16[16,32,2048]{2,1,0:T(8,128)(2,1)}, u32[]{:S(2)}, u32[]{:S(2)}) %all-to-all-start.1) | async-done | bytes 2097184 | tf_op jit(solution)/shard_map/all_to_all | solution.py:135
  201.8 4.2 %gather_fusion = bf16[256,2048]{1,0:T(8,128)(2,1)S(1)} fusion(bf16[512,2048]{1,0:T(8,128)(2,1)} %bitcast.14, s32[1024]{0:T(1024)S(1)} %pad_clamp_fusion), kind=kCustom, calls=%fused_computation | custom fusion | bytes 2098176 | tf_op jit(solution)/shard_map/gather | solution.py:136
  206.1 2.4 %reshape.176 = f32[128,2,2048]{2,1,0:T(2,128)} reshape(bf16[256,2048]{1,0:T(8,128)(2,1)S(1)} %gather_fusion) | data formatting | bytes 3145728 | tf_op jit(solution)/shard_map/convert_element_type | solution.py:139
  208.4 4.9 %multiply_reduce_fusion = f32[128,2048]{1,0:T(8,128)S(1)} fusion(f32[128,2,2048]{2,1,0:T(2,128)} %reshape.176, f32[128,2]{1,0:T(8,128)S(1)} %copy.67), kind=kLoop, calls=%fused_computation.14 | loop fusion | flops 786432 | bytes 3146752 | tf_op jit(solution)/shard_map/reduce_sum | solution.py:139
  213.3 0.9 add_convert_fusion
  (64 shorter events, 0.3 us)
Async XLA Ops:
  7.2 135.7 %copy-start = (bf16[1,512,2048]{2,1,0:T(8,128)(2,1)S(1)}, bf16[1,512,2048]{2,1,0:T(8,128)(2,1)}, u32[]{:S(2)}) copy-start(bf16[1,512,2048]{2,1,0:T(8,128)(2,1)} %param.40) | copy-start | bytes 6291460
  7.2 54.0 %all-gather.2.cloned.1.call-start = ((), (), s32[]{:S(2)}) async-start(), calls=%async_computation.2 | async-start | bytes 4456448 | tf_op jit(solution)/shard_map/all_gather | solution.py:98
  19.0 3.1 %copy-start.6 = (bf16[128,2048]{1,0:T(8,128)(2,1)S(1)}, bf16[128,2048]{1,0:T(8,128)(2,1)}, u32[]{:S(2)}) copy-start(bf16[128,2048]{1,0:T(8,128)(2,1)} %param.21) | copy-start | bytes 1572868
  19.0 3.3 %copy-start.19 = (f32[64,64]{1,0:T(8,128)S(1)}, f32[64,64]{1,0:T(8,128)}, u32[]{:S(2)}) copy-start(f32[64,64]{1,0:T(8,128)} %param.26) | copy-start | bytes 49156
  19.1 3.3 %copy-start.20 = (f32[64,64]{1,0:T(8,128)S(1)}, f32[64,64]{1,0:T(8,128)}, u32[]{:S(2)}) copy-start(f32[64,64]{1,0:T(8,128)} %param.25) | copy-start | bytes 49156
  19.1 42.2 %copy-start.22 = (f32[2048]{0:T(1024)S(1)}, f32[2048]{0:T(1024)}, u32[]{:S(2)}) copy-start(f32[2048]{0:T(1024)} %param.23) | copy-start | bytes 24580
  23.2 43.5 %copy-start.8 = (f32[64,64,16]{1,2,0:T(8,128)S(1)}, f32[64,64,16]{1,2,0:T(8,128)}, u32[]{:S(2)}) copy-start(f32[64,64,16]{1,2,0:T(8,128)} %param.29) | copy-start | bytes 786436
  66.8 5.0 %copy-start.3 = (f32[1,128,4096]{1,2,0:T(8,128)S(1)}, f32[1,128,4096]{1,2,0:T(8,128)}, u32[]{:S(2)}) copy-start(f32[1,128,4096]{1,2,0:T(8,128)} %copy.58) | copy-start | bytes 6291460
  66.8 5.0 %copy-start.4 = (f32[1,128,4096]{1,2,0:T(8,128)S(1)}, f32[1,128,4096]{1,2,0:T(8,128)}, u32[]{:S(2)}) copy-start(f32[1,128,4096]{1,2,0:T(8,128)} %copy.59) | copy-start | bytes 6291460
  66.8 5.0 %copy-start.9 = (f32[64,64,16]{1,2,0:T(8,128)S(1)}, f32[64,64,16]{1,2,0:T(8,128)}, u32[]{:S(2)}) copy-start(f32[64,64,16]{1,2,0:T(8,128)} %param.28) | copy-start | bytes 786436
  66.8 4.9 %copy-start.13 = (f32[64,64]{1,0:T(8,128)S(1)}, f32[64,64]{1,0:T(8,128)}, u32[]{:S(2)}) copy-start(f32[64,64]{1,0:T(8,128)} %get-tuple-element.6) | copy-start | bytes 49156
  66.8 4.9 %copy-start.14 = (f32[64,64]{1,0:T(8,128)S(1)}, f32[64,64]{1,0:T(8,128)}, u32[]{:S(2)}) copy-start(f32[64,64]{1,0:T(8,128)} %get-tuple-element.7) | copy-start | bytes 49156
  66.8 4.9 %copy-start.15 = (f32[64,64]{1,0:T(8,128)S(1)}, f32[64,64]{1,0:T(8,128)}, u32[]{:S(2)}) copy-start(f32[64,64]{1,0:T(8,128)} %get-tuple-element.8) | copy-start | bytes 49156
  66.8 4.9 %copy-start.16 = (f32[64,64]{1,0:T(8,128)S(1)}, f32[64,64]{1,0:T(8,128)}, u32[]{:S(2)}) copy-start(f32[64,64]{1,0:T(8,128)} %get-tuple-element.9) | copy-start | bytes 49156
  71.8 5.2 %copy-start.2 = (f32[128,64,64]{0,2,1:T(8,128)}, f32[128,64,64]{0,2,1:T(8,128)S(1)}, u32[]{:S(2)}) copy-start(f32[128,64,64]{0,2,1:T(8,128)S(1)} %bitcast_add_fusion) | copy-start | bytes 6291460
  71.8 3.3 %copy-start.12 = (f32[64,16,64]{2,1,0:T(8,128)S(1)}, f32[64,16,64]{2,1,0:T(8,128)}, u32[]{:S(2)}) copy-start(f32[64,16,64]{2,1,0:T(8,128)} %param.30) | copy-start | bytes 786436
  75.0 3.9 %copy-start.1 = (f32[128,64,64]{0,2,1:T(8,128)}, f32[128,64,64]{0,2,1:T(8,128)S(1)}, u32[]{:S(2)}) copy-start(f32[128,64,64]{0,2,1:T(8,128)S(1)} %bitcast_add_fusion.1) | copy-start | bytes 6291460
  75.1 1.9 copy-start.11
  77.0 2.9 %copy-start.10 = (bf16[128,1024]{1,0:T(8,128)(2,1)S(1)}, bf16[128,1024]{1,0:T(8,128)(2,1)}, u32[]{:S(2)}) copy-start(bf16[128,1024]{1,0:T(8,128)(2,1)} %convolution_convert_fusion.2) | copy-start | bytes 786436
  77.0 2.9 %copy-start.26 = (f32[1024]{0:T(1024)S(1)}, f32[1024]{0:T(1024)}, u32[]{:S(2)}) copy-start(f32[1024]{0:T(1024)} %param.32) | copy-start | bytes 12292
  79.9 5.6 %copy-start.23 = (f32[2048]{0:T(1024)S(1)}, f32[2048]{0:T(1024)}, u32[]{:S(2)}) copy-start(f32[2048]{0:T(1024)} %param.35) | copy-start | bytes 24580
  87.7 52.9 %copy-start.25 = (bf16[1,2048,512]{2,1,0:T(8,128)(2,1)S(1)}, bf16[1,2048,512]{2,1,0:T(8,128)(2,1)}, u32[]{:S(2)}) copy-start(bf16[1,2048,512]{2,1,0:T(8,128)(2,1)} %param.38) | copy-start | bytes 6291460
  139.3 1.3 copy-start.7
  149.1 5.2 %copy-start.17 = (s32[128,2]{1,0:T(8,128)S(1)}, s32[128,2]{1,0:T(8,128)}, u32[]{:S(2)}) copy-start(s32[128,2]{1,0:T(8,128)} %get-tuple-element.10) | copy-start | bytes 3076
  149.1 5.4 %copy-start.24 = (s32[128,2]{0,1:T(2,128)S(1)}, s32[128,2]{0,1:T(2,128)}, u32[]{:S(2)}) copy-start(s32[128,2]{0,1:T(2,128)} %param.41) | copy-start | bytes 3076
  149.1 5.4 %copy-start.21 = (bf16[2048,4]{0,1:T(4,128)(2,1)S(1)}, bf16[2048,4]{0,1:T(4,128)(2,1)}, u32[]{:S(2)}) copy-start(bf16[2048,4]{0,1:T(4,128)(2,1)} %param.36) | copy-start | bytes 49156
  149.1 5.7 %copy-start.18 = (bf16[2048,16]{0,1:T(8,128)(2,1)S(1)}, bf16[2048,16]{0,1:T(8,128)(2,1)}, u32[]{:S(2)}) copy-start(bf16[2048,16]{0,1:T(8,128)(2,1)} %param.37) | copy-start | bytes 196612
  149.1 52.7 %all-to-all-start.1 = ((bf16[16,32,2048]{2,1,0:T(8,128)(2,1)}), bf16[16,32,2048]{2,1,0:T(8,128)(2,1)}, u32[]{:S(2)}, u32[]{:S(2)}) async-start(bf16[16,32,2048]{2,1,0:T(8,128)(2,1)} %bitcast.81), calls=%async_computation.1 | async-start | bytes 4194304 | tf_op jit(solution)/shard_map/all_to_all | solution.py:135
  208.4 4.9 %copy-start.5 = (f32[128,2048]{1,0:T(8,128)S(1)}, f32[128,2048]{1,0:T(8,128)}, u32[]{:S(2)}) copy-start(f32[128,2048]{1,0:T(8,128)} %get-tuple-element.13) | copy-start | bytes 3145732
Sparse Core Ops, SparseCore 0:
  10.1 51.0 all-gather.1
where the time goes:
time: 222 us; the launch traced here: 221 us
  waiting for transfers between devices  74.7 us (34%)
  blocking collectives  51.6 us (23%)
  matrix products  31.7 us (14%)
  local copies, waits for them, and re-layouts  28.9 us (13%)
  other arithmetic  14.5 us (7%)
  between operations  14.5 us (7%)
  starting transfers between devices  5.21 us (2%)
    all_to_all x1, blocking collectives, on_device(): lax.all_to_all(outgoing, 'ep', split_axis=0, concat_axis=0, tiled=True)  51.6 us
    all_gather x1, waiting for transfers between devices, on_device(): lax.all_gather(w_in, 'ep', axis=1, tiled=True)  38 us
    all_to_all x1, waiting for transfers between devices, on_device(): lax.all_to_all(result, 'ep', split_axis=0, concat_axis=0, tiled=True)  36.1 us
    slice x2, local copies, waits for them, and re-layouts, mixer_step(): old_re = state[0].reshape(rows, groups, entries)  7.65 us
    dot_general x1, matrix products, on_device(): jnp.einsum('erf,efd->erd', inner, w_down, preferred_element_type=jnp.floa...  6.23 us
    another operation x2, local copies, waits for them, and re-layouts, mixer_step(): new_state = jnp.stack([new_re.reshape(rows, -1), new_im.reshape(rows, -1)])  5.82 us
    dot_general x1, matrix products, on_device(): jnp.dot(glu, w_out, preferred_element_type=jnp.float32)  5.62 us
    all_to_all x1, starting transfers between devices, on_device(): lax.all_to_all(result, 'ep', split_axis=0, concat_axis=0, tiled=True)  5.17 us
  transfers between devices with their start and end apart: 2, of which 2 were waited for; matrix products, arithmetic and copies ran while one was open for 12% of the time, Pallas kernels for 0%

commit v1 on v0

v1 whole, which is shorter than its diff:
```python
import functools

import jax
import jax.numpy as jnp
from jax import lax
from jax.experimental import pallas as pl
from jax.experimental.pallas import tpu as pltpu
from jax.sharding import PartitionSpec as P

EXP_GROUPS = 4
TOPK = 2
MESH = pl.DeviceIdType.MESH
VMEM = pl.BlockSpec(memory_space=pltpu.VMEM)
ANY = pl.BlockSpec(memory_space=pl.ANY)
F32 = jnp.float32
BF16 = jnp.bfloat16
NT = (((1,), (1,)), ((), ()))
TN = (((0,), (0,)), ((), ()))
LIMIT = 60 * 1024 * 1024


def remote(src, dst, send_sem, recv_sem, device):
    return pltpu.make_async_remote_copy(
        src_ref=src, dst_ref=dst, send_sem=send_sem, recv_sem=recv_sem, device_id=device, device_id_type=MESH
    )


def greet(peers):
    barrier = pltpu.get_barrier_semaphore()
    for peer in peers:
        pl.semaphore_signal(barrier, inc=1, device_id=peer, device_id_type=MESH)
    pl.semaphore_wait(barrier, len(peers))


def gather_kernel(
    chips, hidden_ref, gain_ref, w_ref, out_ref, held, normed, cw_s, cw_r, cc_s, cc_r, x_s, x_r,
    dcw_s, dcw_r, dcc_s, dcc_r, dx_s, dx_r, own_s, own_r, local_sem,
):
    grp = lax.axis_index("grp")
    me = lax.axis_index("ep")
    chip, core = me // 2, me % 2
    half = chips // 2
    odd = chip % 2
    pos = (chip // 2) * (1 - odd) + (chips - 1 - chip // 2) * odd

    def chip_at(place):
        place = (place + 2 * chips) % chips
        upper = place // half
        return 2 * place * (1 - upper) + (2 * (chips - 1 - place) + 1) * upper

    right = (grp, chip_at(pos + 1) * 2 + core)
    left = (grp, chip_at(pos - 1) * 2 + core)
    mate = (grp, me + 1 - 2 * core)
    side = grp % 2
    across = (grp + 1 - 2 * side, me)
    greet([right, left, mate, across])
    rows, depth = w_ref.shape
    third = depth // 3 // 128 * 128
    cw_cols = pl.ds(third, depth - 2 * third)
    cc_cols = pl.ds(pl.multiple_of(side * (depth - third), 128), third)
    x_cols = pl.ds(pl.multiple_of((1 - side) * (depth - third), 128), third)
    subs = 2
    part = rows // subs

    def piece(origin, sub, cols, own=False, who=core):
        span = pl.ds(sub * part, part)
        return w_ref.at[span, cols] if own else held.at[origin, who, span, cols]

    sends = []

    def start(copy):
        copy.start()
        sends.append(copy)

    def cw(step, sub):
        origin = chip_at(pos - step)
        return remote(piece(origin, sub, cw_cols, step == 0), piece(origin, sub, cw_cols), cw_s.at[step, sub], cw_r.at[step, sub], right)

    def cc(step, sub):
        origin = chip_at(pos + step)
        return remote(piece(origin, sub, cc_cols, step == 0), piece(origin, sub, cc_cols), cc_s.at[step, sub], cc_r.at[step, sub], left)

    def cw_in(step, sub):
        spot = piece(chip_at(pos - step - 1), sub, cw_cols)
        return remote(spot, spot, cw_s.at[step, sub], cw_r.at[step, sub], right)

    def cc_in(step, sub):
        spot = piece(chip_at(pos + step + 1), sub, cc_cols)
        return remote(spot, spot, cc_s.at[step, sub], cc_r.at[step, sub], left)

    for sub in range(subs):
        start(cw(0, sub))
        start(cc(0, sub))
    own = remote(w_ref, held.at[chip, core], own_s, own_r, mate)
    start(own)
    local = pltpu.make_async_copy(w_ref, held.at[chip, core], local_sem)
    local.start()

    wide = hidden_ref[...].astype(F32)
    mean = jnp.mean(wide * wide, axis=-1, keepdims=True)
    normed[...] = (wide * lax.rsqrt(mean + 1e-06) * gain_ref[...]).astype(BF16)

    def take_x(step):
        origin = chip_at(pos + step)
        spot = held.at[origin, core, :, x_cols]
        remote(spot, spot, x_s.at[step], x_r.at[step], across).wait_recv()
        start(remote(spot, spot, dx_s.at[step], dx_r.at[step], mate))

    for step in range(1, chips):
        for sub in range(subs):
            cw_in(step - 1, sub).wait_recv()
            if step < chips - 1:
                start(cw(step, sub))
            spot = piece(chip_at(pos - step), sub, cw_cols)
            start(remote(spot, spot, dcw_s.at[step, sub], dcw_r.at[step, sub], mate))
            cc_in(step - 1, sub).wait_recv()
            if step < chips - 1:
                start(cc(step, sub))
            spot = piece(chip_at(pos + step), sub, cc_cols)
            start(remote(spot, spot, dcc_s.at[step, sub], dcc_r.at[step, sub], mate))
        spot = held.at[chip_at(pos + step), core, :, cc_cols]
        start(remote(spot, spot, x_s.at[step], x_r.at[step], across))
        if step >= 2:
            take_x(step - 1)
    take_x(chips - 1)
    other = 1 - core
    for step in range(1, chips):
        for sub in range(subs):
            spot = piece(chip_at(pos - step), sub, cw_cols, False, other)
            remote(spot, spot, dcw_s.at[step, sub], dcw_r.at[step, sub], mate).wait_recv()
            spot = piece(chip_at(pos + step), sub, cc_cols, False, other)
            remote(spot, spot, dcc_s.at[step, sub], dcc_r.at[step, sub], mate).wait_recv()
        spot = held.at[chip_at(pos + step), other, :, x_cols]
        remote(spot, spot, dx_s.at[step], dx_r.at[step], mate).wait_recv()
    spot = held.at[chip, other]
    remote(spot, spot, own_s, own_r, mate).wait_recv()
    local.wait()
    for pair in range(chips // 2):
        block = held[2 * pair : 2 * pair + 2].reshape(4 * rows, depth)
        product = lax.dot_general(normed[...], block, NT, preferred_element_type=F32)
        out_ref[:, 4 * rows * pair : 4 * rows * (pair + 1)] = product.astype(BF16)
    for copy in sends:
        copy.wait_send()


def mixer_kernel(
    per_group, state_ref, inputs_ref, coef_ref, in_re_ref, in_im_ref, out_re_ref, out_im_ref, skip_ref,
    hidden_ref, gain_ref, w_glu_any, w_out_any, w_logit_ref, ids_ref,
    new_ref, resid_ref, rows_ref, place_ref, active, glu_w, out_w, sems,
):
    step = pl.program_id(0)
    steps = pl.num_programs(0)
    width = inputs_ref.shape[1]
    span = state_ref.shape[2]
    entries = out_re_ref.shape[1]
    channels = in_re_ref.shape[1]
    glu_copy = pltpu.make_async_copy(w_glu_any, glu_w, sems.at[0])
    out_copy = pltpu.make_async_copy(w_out_any, out_w, sems.at[1])

    @pl.when(step == 0)
    def _():
        glu_copy.start()
        out_copy.start()

    def iota(shape, axis):
        return lax.broadcasted_iota(jnp.int32, shape, axis)

    spread_in = (iota((channels, width), 1) % channels == iota((channels, width), 0)).astype(BF16)
    mask_in = iota((span, width), 0) // entries == iota((span, width), 1) // channels
    spread_out = (iota((entries, span), 1) % entries == iota((entries, span), 0)).astype(BF16)
    mask_out = iota((width, span), 0) // channels == iota((width, span), 1) // entries

    def block_in(ref):
        tiled = jnp.dot(ref[...].astype(BF16), spread_in, preferred_element_type=F32)
        return jnp.where(mask_in, tiled, 0.0).astype(BF16)

    def block_out(ref):
        tiled = jnp.dot(ref[...].astype(BF16), spread_out, preferred_element_type=F32)
        return jnp.where(mask_out, tiled, 0.0).astype(BF16)

    inputs = inputs_ref[...]
    drive_re = lax.dot_general(inputs, block_in(in_re_ref), NT, preferred_element_type=F32)
    drive_im = lax.dot_general(inputs, block_in(in_im_ref), NT, preferred_element_type=F32)
    bar_re, bar_im = coef_ref[0:1, :], coef_ref[1:2, :]
    coef_re, coef_im = coef_ref[2:3, :], coef_ref[3:4, :]
    old_re, old_im = state_ref[0], state_ref[1]
    new_re = bar_re * old_re - bar_im * old_im + (coef_re * drive_re - coef_im * drive_im)
    new_im = bar_re * old_im + bar_im * old_re + (coef_re * drive_im + coef_im * drive_re)
    new_ref[0] = new_re
    new_ref[1] = new_im
    read = lax.dot_general(new_re.astype(BF16), block_out(out_re_ref), NT, preferred_element_type=F32)
    read = read - lax.dot_general(new_im.astype(BF16), block_out(out_im_ref), NT, preferred_element_type=F32)
    mixed = read + skip_ref[...] * inputs.astype(F32)
    active[:, pl.ds(pl.multiple_of(step * width, 128), width)] = jax.nn.gelu(mixed)

    @pl.when(step == steps - 1)
    def _():
        glu_copy.wait()
        out_copy.wait()
        act = active[...]
        gating = jnp.dot(act.astype(BF16), glu_w[...], preferred_element_type=F32)
        glu = (act * jax.nn.sigmoid(gating)).astype(BF16)
        resid = (hidden_ref[...].astype(F32) + jnp.dot(glu, out_w[...], preferred_element_type=F32)).astype(BF16)
        resid_ref[...] = resid
        wide = resid.astype(F32)
        mean = jnp.mean(wide * wide, axis=-1, keepdims=True)
        normed = (wide * lax.rsqrt(mean + 1e-06) * gain_ref[...]).astype(BF16)
        depth = normed.shape[1]
        rows_ref[:, :depth] = normed
        logits = jnp.dot(normed, w_logit_ref[...], preferred_element_type=F32)
        count = logits.shape[0]
        lane = iota((count, 128), 1)
        first, second = ids_ref[:, 0:1], ids_ref[:, 1:2]
        group = first // per_group
        own = jnp.sum(jnp.where(lane == group, logits, 0.0), axis=1, keepdims=True)
        scale = 1.0 / jnp.sum(jnp.where(lane < EXP_GROUPS, jnp.exp(jnp.where(lane < EXP_GROUPS, logits - own, 0.0)), 0.0), axis=1, keepdims=True)
        r0 = jnp.sum(jnp.where(lane == first + EXP_GROUPS, logits, 0.0), axis=1, keepdims=True)
        r1 = jnp.sum(jnp.where(lane == second + EXP_GROUPS, logits, 0.0), axis=1, keepdims=True)
        share = jax.nn.sigmoid(r0 - r1)
        member = lane % per_group
        gate = jnp.where(member == first % per_group, scale * share, 0.0)
        gate = gate + jnp.where(member == second % per_group, scale * (1.0 - share), 0.0)
        high = gate.astype(BF16).astype(F32)
        packed = jnp.where(lane < per_group, high, jnp.where(lane < 2 * per_group, gate - high, 0.0))
        rows_ref[:, depth:] = packed.astype(BF16)
        hits = (lane == group).astype(BF16)
        earlier = (iota((count, count), 1) < iota((count, count), 0)).astype(BF16)
        before = jnp.dot(earlier, hits, preferred_element_type=F32)
        rank = jnp.sum(jnp.where(lane == group, before, 0.0), axis=1, keepdims=True).astype(jnp.int32)
        slots = place_ref.shape[1]
        slot = group * (slots // EXP_GROUPS) + rank
        place_ref[...] = (iota((count, slots), 1) == slot).astype(BF16)


def expert_kernel(
    groups, per_group, rows_ref, place_ref, resid_ref, gate_any, up_any, down_any, out_ref,
    outgoing, tokens, parts, parts_in, sums, sums_in, final, returned, w_gate, w_up, w_down,
    zs, zr, ys, yr, cs, cr, ps, pr, qs, qr, bs, br, w_sems,
):
    grp = lax.axis_index("grp")
    me = lax.axis_index("ep")
    pairs = per_group // 2
    g, p = me // per_group, me % per_group
    q, c = p // 2, p % 2
    depth = resid_ref.shape[1]
    cap = outgoing.shape[1]
    wide = outgoing.shape[2]

    def at(group, pair):
        return (grp, group * per_group + pair * 2 + c)

    mate = (grp, me + 1 - 2 * c)
    others = [(g + i) % groups for i in range(1, groups)]
    mates_q = [(q + j) % pairs for j in range(1, pairs)]
    loads = [
        pltpu.make_async_copy(gate_any.at[0], w_gate, w_sems.at[0]),
        pltpu.make_async_copy(up_any.at[0], w_up, w_sems.at[1]),
        pltpu.make_async_copy(down_any.at[0], w_down, w_sems.at[2]),
    ]
    for load in loads:
        load.start()
    sent = lax.dot_general(place_ref[...], rows_ref[...], TN, preferred_element_type=F32).astype(BF16)
    outgoing[...] = sent.reshape(groups, cap, wide)
    tokens[g, c, q] = outgoing[g]
    greet([at(o, q) for o in others] + [at(g, o) for o in mates_q] + [mate])
    sends = []

    def start(copy):
        copy.start()
        sends.append(copy)

    for target in others:
        start(remote(outgoing.at[target], tokens.at[g, c, q], zs.at[target], zr.at[g], at(target, q)))

    def source(i):
        return (g + groups - i) % groups

    def to_mate(s, pair):
        spot = tokens.at[s, c, pair]
        start(remote(spot, spot, cs.at[s, pair], cr.at[s, pair], mate))

    def stage_a(i):
        s = source(i)
        spot = tokens.at[s, c, q]
        if i > 0:
            remote(spot, spot, zs.at[s], zr.at[s], mate).wait_recv()
        for o in mates_q:
            start(remote(spot, spot, ys.at[s, o], yr.at[s, q], at(g, o)))
        to_mate(s, q)

    def stage_b(i):
        s = source(i)
        for o in mates_q:
            spot = tokens.at[s, c, o]
            remote(spot, spot, ys.at[s, o], yr.at[s, o], mate).wait_recv()
            to_mate(s, o)

    def stage_c(i):
        s = source(i)
        for o in range(pairs):
            spot = tokens.at[s, 1 - c, o]
            remote(spot, spot, cs.at[s, o], cr.at[s, o], mate).wait_recv()
        if i == 0:
            for load in loads:
                load.wait()
        total = per_group * cap
        x = tokens[s].reshape(total, wide)
        rows = x[:, :depth]
        gate = jnp.dot(rows, w_gate[...], preferred_element_type=F32)
        upper = jnp.dot(rows, w_up[...], preferred_element_type=F32)
        inner = (jax.nn.silu(gate) * upper).astype(BF16)
        result = jnp.dot(inner, w_down[...], preferred_element_type=F32).astype(BF16)
        lane = lax.broadcasted_iota(jnp.int32, (total, wide - depth), 1)
        mine = (lane == p) | (lane == p + per_group)
        weight = jnp.sum(jnp.where(mine, x[:, depth:].astype(F32), 0.0), axis=1, keepdims=True)
        parts[s] = (result.astype(F32) * weight).astype(BF16).reshape(2, pairs, cap, depth)
        start(remote(parts.at[s, 1 - c], parts_in.at[s], ps.at[s], pr.at[s], mate))

    def stage_d(i):
        s = source(i)
        spot = parts_in.at[s]
        remote(spot, spot, ps.at[s], pr.at[s], mate).wait_recv()
        sums[s] = (parts[s, c].astype(F32) + parts_in[s].astype(F32)).astype(BF16)
        for o in mates_q:
            start(remote(sums.at[s, o], sums_in.at[s, q], qs.at[s, o], qr.at[s, q], at(g, o)))

    def stage_e(i):
        s = source(i)
        total = sums[s, q].astype(F32)
        for o in mates_q:
            spot = sums_in.at[s, o]
            remote(spot, spot, qs.at[s, o], qr.at[s, o], mate).wait_recv()
            total = total + sums_in[s, o].astype(F32)
        if i == 0:
            returned[g] = total.astype(BF16)
        else:
            final[s] = total.astype(BF16)
            start(remote(final.at[s], returned.at[g], bs.at[s], br.at[g], at(s, q)))

    stage_a(0)
    for t in range(groups):
        stage_b(t)
        if t + 1 < groups:
            stage_a(t + 1)
        stage_c(t)
        stage_d(t)
        if t > 0:
            stage_e(t - 1)
    stage_e(groups - 1)
    for o in others:
        spot = returned.at[o]
        remote(spot, spot, bs.at[o], br.at[o], mate).wait_recv()
    back = returned[...].reshape(groups * cap, depth)
    moe = jnp.dot(place_ref[...], back, preferred_element_type=F32)
    out_ref[...] = (resid_ref[...].astype(F32) + moe).astype(BF16)
    for copy in sends:
        copy.wait_send()


def on_device(
    hidden, state, norm_gain, w_in, lam_re, lam_im, log_step, in_re, in_im, out_re, out_im, skip, w_glu, w_out,
    ffn_gain, w_group, w_route, w_gate, w_up, w_down, route_ids,
):
    rows, depth = hidden.shape
    devices = lax.axis_size("ep")
    chips = devices // 2
    shard = w_in.shape[1]
    dma = pltpu.SemaphoreType.DMA
    inputs = pl.pallas_call(
        functools.partial(gather_kernel, chips),
        out_shape=jax.ShapeDtypeStruct((rows, shard * devices), BF16),
        in_specs=[VMEM] * 3,
        out_specs=VMEM,
        scratch_shapes=[pltpu.VMEM((chips, 2, shard, depth), BF16), pltpu.VMEM((rows, depth), BF16)]
        + [dma((chips, 2))] * 4 + [dma((chips,))] * 2 + [dma((chips, 2))] * 4 + [dma((chips,))] * 2
        + [dma, dma, dma],
        compiler_params=pltpu.CompilerParams(collective_id=0, has_side_effects=True, vmem_limit_bytes=LIMIT),
        name="gather_in",
    )(hidden, norm_gain[None, :], w_in.T)

    groups, entries = lam_re.shape
    width = in_re.shape[2]
    flat = groups * entries
    lr, li = lam_re.reshape(1, flat), lam_im.reshape(1, flat)
    step = jnp.exp(jnp.broadcast_to(log_step[:, None], (groups, entries)).reshape(1, flat))
    magnitude = jnp.exp(lr * step)
    bar_re = magnitude * jnp.cos(li * step)
    bar_im = magnitude * jnp.sin(li * step)
    denom = lr * lr + li * li
    lessened = bar_re - 1.0
    coef = jnp.concatenate(
        [bar_re, bar_im, (lessened * lr + bar_im * li) / denom, (bar_im * lr - lessened * li) / denom], axis=0
    )
    experts = w_route.shape[1]
    per_group = experts // EXP_GROUPS
    w_logit = jnp.concatenate(
        [w_group, w_route, jnp.zeros((depth, 128 - EXP_GROUPS - experts), BF16)], axis=1
    )
    cap = 2 * rows // EXP_GROUPS
    block = 128 // width
    span = block * entries
    channels = groups * width
    const = lambda *shape: pl.BlockSpec(shape, lambda i: (0,) * len(shape))
    new_state, resid, packed, place = pl.pallas_call(
        functools.partial(mixer_kernel, per_group),
        grid=(groups // block,),
        out_shape=[
            jax.ShapeDtypeStruct(state.shape, F32),
            jax.ShapeDtypeStruct((rows, depth), BF16),
            jax.ShapeDtypeStruct((rows, depth + 128), BF16),
            jax.ShapeDtypeStruct((rows, EXP_GROUPS * cap), BF16),
        ],
        in_specs=[
            pl.BlockSpec((2, rows, span), lambda i: (0, 0, i)),
            pl.BlockSpec((rows, 128), lambda i: (0, i)),
            pl.BlockSpec((4, span), lambda i: (0, i)),
            pl.BlockSpec((span, width), lambda i: (i, 0)),
            pl.BlockSpec((span, width), lambda i: (i, 0)),
            pl.BlockSpec((128, entries), lambda i: (i, 0)),
            pl.BlockSpec((128, entries), lambda i: (i, 0)),
            pl.BlockSpec((1, 128), lambda i: (0, i)),
            const(rows, depth),
            const(1, depth),
            ANY,
            ANY,
            const(depth, 128),
            const(rows, TOPK),
        ],
        out_specs=[
            pl.BlockSpec((2, rows, span), lambda i: (0, 0, i)),
            const(rows, depth),
            const(rows, depth + 128),
            const(rows, EXP_GROUPS * cap),
        ],
        scratch_shapes=[
            pltpu.VMEM((rows, channels), F32),
            pltpu.VMEM(w_glu.shape, BF16),
            pltpu.VMEM(w_out.shape, BF16),
            dma((2,)),
        ],
        compiler_params=pltpu.CompilerParams(dimension_semantics=("arbitrary",), vmem_limit_bytes=LIMIT),
        name="mixer",
    )(
        state, inputs, coef, in_re.reshape(flat, width), in_im.reshape(flat, width),
        out_re.reshape(channels, entries), out_im.reshape(channels, entries), skip[None, :],
        hidden, ffn_gain[None, :], w_glu, w_out, w_logit, route_ids,
    )

    pairs = per_group // 2
    G = EXP_GROUPS
    hidden_out = pl.pallas_call(
        functools.partial(expert_kernel, G, per_group),
        out_shape=jax.ShapeDtypeStruct((rows, depth), BF16),
        in_specs=[VMEM] * 3 + [ANY] * 3,
        out_specs=VMEM,
        scratch_shapes=[
            pltpu.VMEM((G, cap, depth + 128), BF16),
            pltpu.VMEM((G, 2, pairs, cap, depth + 128), BF16),
            pltpu.VMEM((G, 2, pairs, cap, depth), BF16),
            pltpu.VMEM((G, pairs, cap, depth), BF16),
            pltpu.VMEM((G, pairs, cap, depth), BF16),
            pltpu.VMEM((G, pairs, cap, depth), BF16),
            pltpu.VMEM((G, cap, depth), BF16),
            pltpu.VMEM((G, cap, depth), BF16),
            pltpu.VMEM(w_gate.shape[1:], BF16),
            pltpu.VMEM(w_up.shape[1:], BF16),
            pltpu.VMEM(w_down.shape[1:], BF16),
            dma((G,)), dma((G,)), dma((G, pairs)), dma((G, pairs)), dma((G, pairs)), dma((G, pairs)),
            dma((G,)), dma((G,)), dma((G, pairs)), dma((G, pairs)), dma((G,)), dma((G,)), dma((3,)),
        ],
        compiler_params=pltpu.CompilerParams(collective_id=1, has_side_effects=True, vmem_limit_bytes=LIMIT),
        name="experts",
    )(packed, place, resid, w_gate, w_up, w_down)
    return (hidden_out, new_state)


def solution(mesh):
    return jax.shard_map(
        on_device,
        mesh=mesh,
        in_specs=(
            P(("grp", "ep"), None),
            P(None, ("grp", "ep"), None),
            P(),
            P(None, "ep"),
            P(),
            P(),
            P(),
            P(),
            P(),
            P(),
            P(),
            P(),
            P(),
            P(),
            P(),
            P(),
            P(),
            P("ep", None, None),
            P("ep", None, None),
            P("ep", None, None),
            P(("grp", "ep"), None),
        ),
        out_specs=(P(("grp", "ep"), None), P(None, ("grp", "ep"), None)),
        check_vma=False,
    )
```

time: 222 us -> 137 us (0.62)
  the two profiles are of different devices: /device:TPU:13 before, /device:TPU:0 now
where the time goes in v1:
time: 137 us
  Pallas kernels  122 us (89%)
  local copies, waits for them, and re-layouts  11.2 us (8%)
  other arithmetic  2.36 us (2%)
    pallas_call x1, Pallas kernels, on_device(): pl.pallas_call(functools.partial(expert_kernel, G, per_group), out_shape=...  70.4 us
    pallas_call x1, Pallas kernels, on_device(): pl.pallas_call(functools.partial(gather_kernel, chips), out_shape=jax.Sha...  37.6 us
    pallas_call x1, Pallas kernels, on_device(): pl.pallas_call(functools.partial(mixer_kernel, per_group), grid=(groups /...  14.4 us
    unnamed x12, local copies, waits for them, and re-layouts  8.5 us

profile of v1, /device:TPU:0, one launch (start us, length us, event | category | flops | bytes accessed | tf_op | source)
XLA Modules:
  0.0 136.6 jit_solution(3139386195395461411)
XLA Ops:
  0.6 0.0 copy-start.2
  0.6 0.7 exp.50
  1.3 0.1 pad.2.clone
  1.4 0.8 reshape.221
  2.3 0.0 copy-start
  2.3 0.9 reshape.222
  3.2 0.1 broadcast_in_dim.19
  3.3 0.1 exp.51
  3.3 0.5 cosine_multiply_fusion
  3.9 0.7 pad_maximum_fusion.coef_ref
  4.6 1.4 %copy.27.ids_ref = s32[128,2]{1,0:T(8,128)} copy(s32[128,2]{0,1:T(2,128)} %param.41) | data formatting | bytes 2048 | tf_op args[20]
  6.0 37.6 %gather_in.1.inputs_ref = bf16[128,1024]{1,0:T(8,128)(2,1)} custom-call(bf16[128,2048]{1,0:T(8,128)(2,1)} %hidden_ref.3, f32[1,2048]{1,0:T(1,128)} %bitcast.13, bf16[64,2048]{1,0:T(8,128)(2,1)} %bitcast.12), custom_call_target="tpu_custom_call" | custom-call | tf_op jit(solution)/shard_map/gather_in/pallas_call | solution.py:369
  43.6 1.0 copy.25
  44.7 0.0 copy-done.2
  44.7 0.3 copy.26
  44.9 0.0 copy-start.1
  45.0 1.1 maximum_maximum_fusion.w_logit_ref
  46.1 0.0 copy-done
  46.1 2.0 %copy.23 = f32[64,64,16]{2,1,0:T(8,128)} copy(f32[64,64,16]{1,2,0:T(8,128)S(1)} %copy-done) | data formatting | bytes 524288 | tf_op args[7]
  48.0 0.0 copy-done.1
  48.0 1.9 %copy.24 = f32[64,64,16]{2,1,0:T(8,128)} copy(f32[64,64,16]{1,2,0:T(8,128)S(1)} %copy-done.1) | data formatting | bytes 524288 | tf_op args[8]
  50.0 14.4 %mixer.1 = (f32[2,128,4096]{2,1,0:T(8,128)}, bf16[128,2048]{1,0:T(8,128)(2,1)}, bf16[128,2176]{1,0:T(8,128)(2,1)}, bf16[128,256]{1,0:T(8,128)(2,1)}) custom-call(f32[2,128,4096]{2,1,0:T(8,128)} %state_ref.1, bf16[128,1024]{1,0:T(8,128)(2,1)} %gather_in.1.inputs_ref, f32[4,4096]{1,0:T(4,128)} %pad_maximum_fusion.coef_ref, f32[4096,16]{1,0:T(8,128)} %bitcast.8, ...), custom_call_target="tpu_custom_call" | custom-call | tf_op jit(solution)/shard_map/mixer/pallas_call | solution.py:404
  64.4 70.4 %experts.1 = bf16[128,2048]{1,0:T(8,128)(2,1)} custom-call(bf16[128,2176]{1,0:T(8,128)(2,1)} %get-tuple-element.6.rows_ref, bf16[128,256]{1,0:T(8,128)(2,1)} %get-tuple-element.7.place_ref, bf16[128,2048]{1,0:T(8,128)(2,1)} %get-tuple-element.8.resid_ref, bf16[1,2048,512]{2,1,0:T(8,128)(2,1)} %gate_any.1, bf16[1,2048,512]{2,1,0:T(8,128)(2,1)} %up_any.1, ...), custom_call_target="tpu_custom_call" | custom-call | tf_op jit(solution)/shard_map/experts/pallas_call | solution.py:451
  134.7 1.9 %copy.29 = bf16[128,2048]{1,0:T(8,128)(2,1)} copy(bf16[128,2048]{1,0:T(8,128)(2,1)} %experts.1) | data formatting | bytes 1048576
  (1 shorter events, 0.0 us)
Async XLA Ops:
  0.6 44.0 %copy-start.2 = (bf16[2048,16]{0,1:T(8,128)(2,1)S(1)}, bf16[2048,16]{0,1:T(8,128)(2,1)}, u32[]{:S(2)}) copy-start(bf16[2048,16]{0,1:T(8,128)(2,1)} %param.37) | copy-start | bytes 196612
  2.3 43.8 %copy-start = (f32[64,64,16]{1,2,0:T(8,128)S(1)}, f32[64,64,16]{1,2,0:T(8,128)}, u32[]{:S(2)}) copy-start(f32[64,64,16]{1,2,0:T(8,128)} %param.28) | copy-start | bytes 786436
  44.9 3.1 %copy-start.1 = (f32[64,64,16]{1,2,0:T(8,128)S(1)}, f32[64,64,16]{1,2,0:T(8,128)}, u32[]{:S(2)}) copy-start(f32[64,64,16]{1,2,0:T(8,128)} %param.29) | copy-start | bytes 786436

commit v2 on v1

--- a/solution.py
+++ b/solution.py
@@ -33,106 +33,93 @@
 
 
 def gather_kernel(
-    chips, hidden_ref, gain_ref, w_ref, out_ref, held, normed, cw_s, cw_r, cc_s, cc_r, x_s, x_r,
-    dcw_s, dcw_r, dcc_s, dcc_r, dx_s, dx_r, own_s, own_r, local_sem,
+    chips, hidden_ref, gain_ref, w_ref, out_ref, held, normed, zs, zr, ys, yr, xs, xr, ds, dr, es, er,
+    own_s, own_r, local_sem,
 ):
     grp = lax.axis_index("grp")
     me = lax.axis_index("ep")
     chip, core = me // 2, me % 2
-    half = chips // 2
-    odd = chip % 2
-    pos = (chip // 2) * (1 - odd) + (chips - 1 - chip // 2) * odd
-
-    def chip_at(place):
-        place = (place + 2 * chips) % chips
-        upper = place // half
-        return 2 * place * (1 - upper) + (2 * (chips - 1 - place) + 1) * upper
-
-    right = (grp, chip_at(pos + 1) * 2 + core)
-    left = (grp, chip_at(pos - 1) * 2 + core)
+    lines = chips // 2
+    line, y = chip // 2, chip % 2
+
+    def at(row, column):
+        return (grp, (row * 2 + column) * 2 + core)
+
+    targets = [(line + i) % lines for i in range(1, lines)]
     mate = (grp, me + 1 - 2 * core)
     side = grp % 2
     across = (grp + 1 - 2 * side, me)
-    greet([right, left, mate, across])
+    beside = at(line, 1 - y)
     rows, depth = w_ref.shape
     third = depth // 3 // 128 * 128
-    cw_cols = pl.ds(third, depth - 2 * third)
-    cc_cols = pl.ds(pl.multiple_of(side * (depth - third), 128), third)
-    x_cols = pl.ds(pl.multiple_of((1 - side) * (depth - third), 128), third)
+    my_cols = pl.ds(pl.multiple_of(side * third, 128), depth - third)
+    out_cols = pl.ds(pl.multiple_of(side * (depth - third), 128), third)
+    in_cols = pl.ds(pl.multiple_of((1 - side) * (depth - third), 128), third)
     subs = 2
     part = rows // subs
-
-    def piece(origin, sub, cols, own=False, who=core):
-        span = pl.ds(sub * part, part)
-        return w_ref.at[span, cols] if own else held.at[origin, who, span, cols]
-
+    spans = [pl.ds(sub * part, part) for sub in range(subs)]
     sends = []
 
     def start(copy):
         copy.start()
         sends.append(copy)
 
-    def cw(step, sub):
-        origin = chip_at(pos - step)
-        return remote(piece(origin, sub, cw_cols, step == 0), piece(origin, sub, cw_cols), cw_s.at[step, sub], cw_r.at[step, sub], right)
-
-    def cc(step, sub):
-        origin = chip_at(pos + step)
-        return remote(piece(origin, sub, cc_cols, step == 0), piece(origin, sub, cc_cols), cc_s.at[step, sub], cc_r.at[step, sub], left)
-
-    def cw_in(step, sub):
-        spot = piece(chip_at(pos - step - 1), sub, cw_cols)
-        return remote(spot, spot, cw_s.at[step, sub], cw_r.at[step, sub], right)
-
-    def cc_in(step, sub):
-        spot = piece(chip_at(pos + step + 1), sub, cc_cols)
-        return remote(spot, spot, cc_s.at[step, sub], cc_r.at[step, sub], left)
-
-    for sub in range(subs):
-        start(cw(0, sub))
-        start(cc(0, sub))
-    own = remote(w_ref, held.at[chip, core], own_s, own_r, mate)
-    start(own)
     local = pltpu.make_async_copy(w_ref, held.at[chip, core], local_sem)
     local.start()
+    greet([at(target, y) for target in targets] + [beside, mate, across])
+    for i in range(lines):
+        for sub in range(subs):
+            src, dst = w_ref.at[spans[sub], my_cols], held.at[chip, core, spans[sub], my_cols]
+            if i == 0:
+                start(remote(src, dst, ys.at[0, sub], yr.at[0, sub], beside))
+            else:
+                start(remote(src, dst, zs.at[i, sub], zr.at[i, sub], at(targets[i - 1], y)))
+    start(remote(w_ref, held.at[chip, core], own_s, own_r, mate))
 
     wide = hidden_ref[...].astype(F32)
     mean = jnp.mean(wide * wide, axis=-1, keepdims=True)
     normed[...] = (wide * lax.rsqrt(mean + 1e-06) * gain_ref[...]).astype(BF16)
 
-    def take_x(step):
-        origin = chip_at(pos + step)
-        spot = held.at[origin, core, :, x_cols]
-        remote(spot, spot, x_s.at[step], x_r.at[step], across).wait_recv()
-        start(remote(spot, spot, dx_s.at[step], dx_r.at[step], mate))
-
-    for step in range(1, chips):
+    def origin(kind, i):
+        return (line + lines - i) % lines * 2 + (y if kind == 0 else 1 - y)
+
+    order = []
+    for i in range(1, lines + 1):
         for sub in range(subs):
-            cw_in(step - 1, sub).wait_recv()
-            if step < chips - 1:
-                start(cw(step, sub))
-            spot = piece(chip_at(pos - step), sub, cw_cols)
-            start(remote(spot, spot, dcw_s.at[step, sub], dcw_r.at[step, sub], mate))
-            cc_in(step - 1, sub).wait_recv()
-            if step < chips - 1:
-                start(cc(step, sub))
-            spot = piece(chip_at(pos + step), sub, cc_cols)
-            start(remote(spot, spot, dcc_s.at[step, sub], dcc_r.at[step, sub], mate))
-        spot = held.at[chip_at(pos + step), core, :, cc_cols]
-        start(remote(spot, spot, x_s.at[step], x_r.at[step], across))
-        if step >= 2:
-            take_x(step - 1)
-    take_x(chips - 1)
-    other = 1 - core
-    for step in range(1, chips):
-        for sub in range(subs):
-            spot = piece(chip_at(pos - step), sub, cw_cols, False, other)
-            remote(spot, spot, dcw_s.at[step, sub], dcw_r.at[step, sub], mate).wait_recv()
-            spot = piece(chip_at(pos + step), sub, cc_cols, False, other)
-            remote(spot, spot, dcc_s.at[step, sub], dcc_r.at[step, sub], mate).wait_recv()
-        spot = held.at[chip_at(pos + step), other, :, x_cols]
-        remote(spot, spot, dx_s.at[step], dx_r.at[step], mate).wait_recv()
-    spot = held.at[chip, other]
+            if i < lines:
+                order.append((0, i, sub))
+            order.append((1, i - 1, sub))
+
+    def take(kind, i, sub):
+        place = origin(kind, i)
+        spot = held.at[place, core, spans[sub], my_cols]
+        if kind == 0:
+            remote(spot, spot, zs.at[i, sub], zr.at[i, sub], mate).wait_recv()
+            start(remote(spot, spot, ys.at[i, sub], yr.at[i, sub], beside))
+        else:
+            remote(spot, spot, ys.at[i, sub], yr.at[i, sub], mate).wait_recv()
+        side_spot = held.at[place, core, spans[sub], out_cols]
+        start(remote(side_spot, side_spot, xs.at[kind, i, sub], xr.at[kind, i, sub], across))
+        start(remote(spot, spot, ds.at[kind, i, sub], dr.at[kind, i, sub], mate))
+
+    def take_x(kind, i, sub):
+        spot = held.at[origin(kind, i), core, spans[sub], in_cols]
+        remote(spot, spot, xs.at[kind, i, sub], xr.at[kind, i, sub], mate).wait_recv()
+        start(remote(spot, spot, es.at[kind, i, sub], er.at[kind, i, sub], mate))
+
+    lag = 2 * subs
+    for at_ in range(len(order) + lag):
+        if at_ < len(order):
+            take(*order[at_])
+        if at_ >= lag:
+            take_x(*order[at_ - lag])
+    for kind, i, sub in order:
+        place = origin(kind, i)
+        spot = held.at[place, 1 - core, spans[sub], my_cols]
+        remote(spot, spot, ds.at[kind, i, sub], dr.at[kind, i, sub], mate).wait_recv()
+        spot = held.at[place, 1 - core, spans[sub], in_cols]
+        remote(spot, spot, es.at[kind, i, sub], er.at[kind, i, sub], mate).wait_recv()
+    spot = held.at[chip, 1 - core]
     remote(spot, spot, own_s, own_r, mate).wait_recv()
     local.wait()
     for pair in range(chips // 2):
@@ -145,7 +132,7 @@
 
 def mixer_kernel(
     per_group, state_ref, inputs_ref, coef_ref, in_re_ref, in_im_ref, out_re_ref, out_im_ref, skip_ref,
-    hidden_ref, gain_ref, w_glu_any, w_out_any, w_logit_ref, ids_ref,
+    hidden_ref, gain_ref, w_glu_any, w_out_any, w_group_ref, w_route_ref, ids_ref,
     new_ref, resid_ref, rows_ref, place_ref, active, glu_w, out_w, sems,
 ):
     step = pl.program_id(0)
@@ -153,7 +140,7 @@
     width = inputs_ref.shape[1]
     span = state_ref.shape[2]
     entries = out_re_ref.shape[1]
-    channels = in_re_ref.shape[1]
+    channels = width // (span // entries)
     glu_copy = pltpu.make_async_copy(w_glu_any, glu_w, sems.at[0])
     out_copy = pltpu.make_async_copy(w_out_any, out_w, sems.at[1])
 
@@ -165,22 +152,16 @@
     def iota(shape, axis):
         return lax.broadcasted_iota(jnp.int32, shape, axis)
 
-    spread_in = (iota((channels, width), 1) % channels == iota((channels, width), 0)).astype(BF16)
-    mask_in = iota((span, width), 0) // entries == iota((span, width), 1) // channels
     spread_out = (iota((entries, span), 1) % entries == iota((entries, span), 0)).astype(BF16)
     mask_out = iota((width, span), 0) // channels == iota((width, span), 1) // entries
 
-    def block_in(ref):
-        tiled = jnp.dot(ref[...].astype(BF16), spread_in, preferred_element_type=F32)
-        return jnp.where(mask_in, tiled, 0.0).astype(BF16)
-
-    def block_out(ref):
+    def block(ref):
         tiled = jnp.dot(ref[...].astype(BF16), spread_out, preferred_element_type=F32)
         return jnp.where(mask_out, tiled, 0.0).astype(BF16)
 
     inputs = inputs_ref[...]
-    drive_re = lax.dot_general(inputs, block_in(in_re_ref), NT, preferred_element_type=F32)
-    drive_im = lax.dot_general(inputs, block_in(in_im_ref), NT, preferred_element_type=F32)
+    drive_re = jnp.dot(inputs, block(in_re_ref), preferred_element_type=F32)
+    drive_im = jnp.dot(inputs, block(in_im_ref), preferred_element_type=F32)
     bar_re, bar_im = coef_ref[0:1, :], coef_ref[1:2, :]
     coef_re, coef_im = coef_ref[2:3, :], coef_ref[3:4, :]
     old_re, old_im = state_ref[0], state_ref[1]
@@ -188,8 +169,8 @@
     new_im = bar_re * old_im + bar_im * old_re + (coef_re * drive_im + coef_im * drive_re)
     new_ref[0] = new_re
     new_ref[1] = new_im
-    read = lax.dot_general(new_re.astype(BF16), block_out(out_re_ref), NT, preferred_element_type=F32)
-    read = read - lax.dot_general(new_im.astype(BF16), block_out(out_im_ref), NT, preferred_element_type=F32)
+    read = lax.dot_general(new_re.astype(BF16), block(out_re_ref), NT, preferred_element_type=F32)
+    read = read - lax.dot_general(new_im.astype(BF16), block(out_im_ref), NT, preferred_element_type=F32)
     mixed = read + skip_ref[...] * inputs.astype(F32)
     active[:, pl.ds(pl.multiple_of(step * width, 128), width)] = jax.nn.gelu(mixed)
 
@@ -207,15 +188,18 @@
         normed = (wide * lax.rsqrt(mean + 1e-06) * gain_ref[...]).astype(BF16)
         depth = normed.shape[1]
         rows_ref[:, :depth] = normed
-        logits = jnp.dot(normed, w_logit_ref[...], preferred_element_type=F32)
-        count = logits.shape[0]
+        level = lax.dot_general(normed, w_group_ref[...], NT, preferred_element_type=F32)
+        logits = lax.dot_general(normed, w_route_ref[...], NT, preferred_element_type=F32)
+        count = normed.shape[0]
         lane = iota((count, 128), 1)
-        first, second = ids_ref[:, 0:1], ids_ref[:, 1:2]
+        same = (iota((count, count), 0) == iota((count, count), 1)).astype(BF16)
+        ids = lax.dot_general(same, ids_ref[...].astype(F32).astype(BF16), NT, preferred_element_type=F32).astype(jnp.int32)
+        first, second = ids[:, 0:1], ids[:, 1:2]
         group = first // per_group
-        own = jnp.sum(jnp.where(lane == group, logits, 0.0), axis=1, keepdims=True)
-        scale = 1.0 / jnp.sum(jnp.where(lane < EXP_GROUPS, jnp.exp(jnp.where(lane < EXP_GROUPS, logits - own, 0.0)), 0.0), axis=1, keepdims=True)
-        r0 = jnp.sum(jnp.where(lane == first + EXP_GROUPS, logits, 0.0), axis=1, keepdims=True)
-        r1 = jnp.sum(jnp.where(lane == second + EXP_GROUPS, logits, 0.0), axis=1, keepdims=True)
+        own = jnp.sum(jnp.where(iota(level.shape, 1) == group, level, 0.0), axis=1, keepdims=True)
+        scale = 1.0 / jnp.sum(jnp.exp(level - own), axis=1, keepdims=True)
+        r0 = jnp.sum(jnp.where(iota(logits.shape, 1) == first, logits, 0.0), axis=1, keepdims=True)
+        r1 = jnp.sum(jnp.where(iota(logits.shape, 1) == second, logits, 0.0), axis=1, keepdims=True)
         share = jax.nn.sigmoid(r0 - r1)
         member = lane % per_group
         gate = jnp.where(member == first % per_group, scale * share, 0.0)
@@ -372,8 +356,7 @@
         in_specs=[VMEM] * 3,
         out_specs=VMEM,
         scratch_shapes=[pltpu.VMEM((chips, 2, shard, depth), BF16), pltpu.VMEM((rows, depth), BF16)]
-        + [dma((chips, 2))] * 4 + [dma((chips,))] * 2 + [dma((chips, 2))] * 4 + [dma((chips,))] * 2
-        + [dma, dma, dma],
+        + [dma((chips // 2, 2))] * 4 + [dma((2, chips // 2, 2))] * 6 + [dma, dma, dma],
         compiler_params=pltpu.CompilerParams(collective_id=0, has_side_effects=True, vmem_limit_bytes=LIMIT),
         name="gather_in",
     )(hidden, norm_gain[None, :], w_in.T)
@@ -393,9 +376,6 @@
     )
     experts = w_route.shape[1]
     per_group = experts // EXP_GROUPS
-    w_logit = jnp.concatenate(
-        [w_group, w_route, jnp.zeros((depth, 128 - EXP_GROUPS - experts), BF16)], axis=1
-    )
     cap = 2 * rows // EXP_GROUPS
     block = 128 // width
     span = block * entries
@@ -414,8 +394,8 @@
             pl.BlockSpec((2, rows, span), lambda i: (0, 0, i)),
             pl.BlockSpec((rows, 128), lambda i: (0, i)),
             pl.BlockSpec((4, span), lambda i: (0, i)),
-            pl.BlockSpec((span, width), lambda i: (i, 0)),
-            pl.BlockSpec((span, width), lambda i: (i, 0)),
+            pl.BlockSpec((128, entries), lambda i: (i, 0)),
+            pl.BlockSpec((128, entries), lambda i: (i, 0)),
             pl.BlockSpec((128, entries), lambda i: (i, 0)),
             pl.BlockSpec((128, entries), lambda i: (i, 0)),
             pl.BlockSpec((1, 128), lambda i: (0, i)),
@@ -423,8 +403,9 @@
             const(1, depth),
             ANY,
             ANY,
-            const(depth, 128),
-            const(rows, TOPK),
+            const(EXP_GROUPS, depth),
+            const(experts, depth),
+            const(TOPK, rows),
         ],
         out_specs=[
             pl.BlockSpec((2, rows, span), lambda i: (0, 0, i)),
@@ -441,9 +422,10 @@
         compiler_params=pltpu.CompilerParams(dimension_semantics=("arbitrary",), vmem_limit_bytes=LIMIT),
         name="mixer",
     )(
-        state, inputs, coef, in_re.reshape(flat, width), in_im.reshape(flat, width),
+        state, inputs, coef, in_re.transpose(0, 2, 1).reshape(channels, entries),
+        in_im.transpose(0, 2, 1).reshape(channels, entries),
         out_re.reshape(channels, entries), out_im.reshape(channels, entries), skip[None, :],
-        hidden, ffn_gain[None, :], w_glu, w_out, w_logit, route_ids,
+        hidden, ffn_gain[None, :], w_glu, w_out, w_group.T, w_route.T, route_ids.T,
     )
 
     pairs = per_group // 2

time: 137 us -> 129 us (0.942)
  local copies, waits for them, and re-layouts: 11.2 us -> 4.39 us
    unnamed x12 -> x1, local copies, waits for them, and re-layouts: 8.5 us -> 1.88 us
    pallas_call x1, Pallas kernels: 70.4 us -> 74 us  [on_device(): pl.pallas_call(functools.partial(expert_kernel, G, per_group), out_shape=...]
    pallas_call x1, Pallas kernels: 37.6 us -> 34.2 us  [on_device(): pl.pallas_call(functools.partial(gather_kernel, chips), out_shape=jax.Sha...]
where the time goes in v2:
time: 129 us
  Pallas kernels  123 us (95%)
  local copies, waits for them, and re-layouts  4.39 us (3%)
    pallas_call x1, Pallas kernels, on_device(): pl.pallas_call(functools.partial(expert_kernel, G, per_group), out_shape=...  74 us
    pallas_call x1, Pallas kernels, on_device(): pl.pallas_call(functools.partial(gather_kernel, chips), out_shape=jax.Sha...  34.2 us
    pallas_call x1, Pallas kernels, on_device(): pl.pallas_call(functools.partial(mixer_kernel, per_group), grid=(groups /...  14.3 us

profile of v2, /device:TPU:0, one launch (start us, length us, event | category | flops | bytes accessed | tf_op | source)
XLA Modules:
  0.0 128.8 jit_solution(12092189522332018498)
XLA Ops:
  0.6 0.7 exp.50
  1.3 0.8 reshape.221
  2.1 0.8 reshape.222
  3.0 0.1 broadcast_in_dim.16
  3.1 0.1 exp.51
  3.2 0.5 cosine_multiply_fusion
  3.7 0.7 pad_maximum_fusion.coef_ref
  4.4 34.2 %gather_in.1.inputs_ref = bf16[128,1024]{1,0:T(8,128)(2,1)} custom-call(bf16[128,2048]{1,0:T(8,128)(2,1)} %hidden_ref.3, f32[1,2048]{1,0:T(1,128)} %bitcast.22, bf16[64,2048]{1,0:T(8,128)(2,1)} %bitcast.19), custom_call_target="tpu_custom_call" | custom-call | tf_op jit(solution)/shard_map/gather_in/pallas_call | solution.py:353
  38.6 14.3 %mixer.1 = (f32[2,128,4096]{2,1,0:T(8,128)}, bf16[128,2048]{1,0:T(8,128)(2,1)}, bf16[128,2176]{1,0:T(8,128)(2,1)}, bf16[128,256]{1,0:T(8,128)(2,1)}) custom-call(f32[2,128,4096]{2,1,0:T(8,128)} %state_ref.1, bf16[128,1024]{1,0:T(8,128)(2,1)} %gather_in.1.inputs_ref, f32[4,4096]{1,0:T(4,128)} %pad_maximum_fusion.coef_ref, f32[1024,64]{1,0:T(8,128)} %bitcast.15, ...), custom_call_target="tpu_custom_call" | custom-call | tf_op jit(solution)/shard_map/mixer/pallas_call | solution.py:384
  52.9 74.0 %experts.1 = bf16[128,2048]{1,0:T(8,128)(2,1)} custom-call(bf16[128,2176]{1,0:T(8,128)(2,1)} %get-tuple-element.6.rows_ref, bf16[128,256]{1,0:T(8,128)(2,1)} %get-tuple-element.7.place_ref, bf16[128,2048]{1,0:T(8,128)(2,1)} %get-tuple-element.8.resid_ref, bf16[1,2048,512]{2,1,0:T(8,128)(2,1)} %gate_any.1, bf16[1,2048,512]{2,1,0:T(8,128)(2,1)} %up_any.1, ...), custom_call_target="tpu_custom_call" | custom-call | tf_op jit(solution)/shard_map/experts/pallas_call | solution.py:433
  126.9 1.9 %copy.24 = bf16[128,2048]{1,0:T(8,128)(2,1)} copy(bf16[128,2048]{1,0:T(8,128)(2,1)} %experts.1) | data formatting | bytes 1048576
